TPU v7x, 32 devices: a whole 2x2x4 slice. The times are simulated.
32 devices in a mesh: sp: 16 (over z, y, x), tp: 2 (over core).
Axes of the slice: x: 2, y: 2, z: 4, core: 2. Of those that a mesh axis runs over, the one named last changes fastest.
Arguments:
- latent: bfloat16 [4096, 2048], P(('sp', 'tp')), may hold values from -3 to 3
- context: bfloat16 [1024, 2048], P('sp'), may hold values from -6 to 6
- condition: float32 [2048], replicated, may hold values from -6 to 6
- ctx_cond: float32 [2048], replicated, may hold values from -6 to 6
- norm_gain: float32 [2048], replicated, may hold values from 0.1 to 1.9
- w_shift: bfloat16 [2048, 2048], P('sp', 'tp'), may hold values from -0.25 to 0.25
- w_scale: bfloat16 [2048, 2048], P('sp', 'tp'), may hold values from -0.25 to 0.25
- w_gate: bfloat16 [2048, 2048], P('sp', 'tp'), may hold values from -0.25 to 0.25
- w_query: bfloat16 [2048, 2048], P(None, 'tp'), may hold values from -0.125 to 0.125
- w_key: bfloat16 [2048, 2048], P(None, 'tp'), may hold values from -0.125 to 0.125
- w_value: bfloat16 [2048, 2048], P(None, 'tp'), may hold values from -0.125 to 0.125
- w_out: bfloat16 [2048, 2048], P('tp'), may hold values from -0.125 to 0.125
- rel_bias: float32 [16, 15, 31], replicated, may hold values from 2 to 250
Outputs:
- updated: bfloat16 [4096, 2048], P(('sp', 'tp'))
All inputs are finite; a program needn't handle non-finite values.
Results may differ from a plain program's by a relative error of at most 0.015.
Values may be sent and summed in bfloat16 or wider, within the bound.
A program may use at most 128 MiB of HBM per device.

v0:
```python
import jax
import jax.numpy as jnp
from jax import lax
from jax.sharding import PartitionSpec as P

HEADS = 16
HEAD_DIM = 128
GRID_W = 32
WIN_H = 8
WIN_W = 16


NORM_EPS = 1e-06
NEG_BIG = -1e30


def padded_2(cells, sides, width):
    for axis, dim in sides:
        count = lax.axis_size(axis)
        ends = count - 1
        head = lax.slice_in_dim(cells, 0, width, axis=dim)
        tail = lax.slice_in_dim(cells, cells.shape[dim] - width, cells.shape[dim], axis=dim)
        cells = jnp.concatenate(
            [
                lax.ppermute(tail, axis, [(i, (i + 1) % count) for i in range(ends)]),
                cells,
                lax.ppermute(head, axis, [((i + 1) % count, i) for i in range(ends)]),
            ],
            axis=dim,
        )
    return cells


def rms_mod(block, norm_gain, shifts, scales):
    block = block.astype(jnp.float32)
    normed = (
        block * lax.rsqrt(jnp.mean(block * block, axis=-1, keepdims=True) + NORM_EPS) * norm_gain
    )
    return (normed * (1.0 + scales) + shifts).astype(jnp.bfloat16)


def project(block, weights):
    return jnp.stack(
        [
            jnp.dot(block, weight, preferred_element_type=jnp.float32).astype(jnp.bfloat16)
            for weight in weights
        ]
    )


def on_device(
    latent,
    context,
    condition,
    ctx_cond,
    norm_gain,
    w_shift,
    w_scale,
    w_gate,
    w_query,
    w_key,
    w_value,
    w_out,
    rel_bias,
):
    tp_size = lax.axis_size("tp")
    sp_size = lax.axis_size("sp")
    head_dev = HEADS // tp_size
    head_cols = w_query.shape[1]
    model_width = w_query.shape[0]
    row_part = w_shift.shape[0]
    col_part = w_shift.shape[1]
    activated = jax.nn.silu(jnp.stack([condition, ctx_cond])).astype(jnp.bfloat16)
    act_rows = lax.dynamic_slice_in_dim(activated, lax.axis_index("sp") * row_part, row_part, 1)
    partial_value = jnp.concatenate(
        [
            jnp.dot(act_rows, w_shift, preferred_element_type=jnp.float32),
            jnp.dot(act_rows, w_scale, preferred_element_type=jnp.float32),
            jnp.dot(act_rows[:1], w_gate, preferred_element_type=jnp.float32),
        ],
        axis=0,
    )
    placed = lax.dynamic_update_slice_in_dim(
        jnp.zeros((5, model_width), jnp.float32), partial_value, lax.axis_index("tp") * col_part, 1
    )
    mod_vecs = lax.psum(placed, ("sp", "tp"))
    normed = rms_mod(latent, norm_gain, mod_vecs[0], mod_vecs[2])
    projected = project(lax.all_gather(normed, "tp", axis=0, tiled=True), (w_query, w_key, w_value))
    ctx_kv = lax.all_gather(
        project(rms_mod(context, norm_gain, mod_vecs[1], mod_vecs[3]), (w_key, w_value)),
        "sp",
        axis=1,
        tiled=True,
    )
    ctx_key3 = ctx_kv[0].reshape(-1, head_dev, HEAD_DIM)
    ctx_val3 = ctx_kv[1].reshape(-1, head_dev, HEAD_DIM)
    grid_rows = projected.shape[1] // GRID_W
    queries = projected[0].reshape(grid_rows, GRID_W, head_dev, HEAD_DIM)
    half_win = WIN_H // 2
    padded = padded_2(
        projected[1:].reshape(2, grid_rows, GRID_W, head_cols), (("sp", 1),), half_win
    )
    total_rows = grid_rows * sp_size
    first_row = lax.axis_index("sp") * grid_rows
    local_rows = jnp.arange(grid_rows, dtype=jnp.int32)
    starts = (
        jnp.clip(first_row + local_rows - half_win, 0, total_rows - WIN_H) - first_row + half_win
    )

    def take_window(start_row):
        return lax.dynamic_slice_in_dim(padded, start_row, WIN_H, 1)

    windows = jax.vmap(take_window)(starts)
    key_win = windows[:, 0].reshape(grid_rows, WIN_H, GRID_W, head_dev, HEAD_DIM)
    val_win = windows[:, 1].reshape(grid_rows, WIN_H, GRID_W, head_dev, HEAD_DIM)
    row_off = (
        starts[:, None]
        - half_win
        + jnp.arange(WIN_H, dtype=jnp.int32)[None, :]
        - local_rows[:, None]
        + WIN_H
        - 1
    )
    col_ids = jnp.arange(GRID_W, dtype=jnp.int32)
    col_start = jnp.clip(col_ids - WIN_W // 2, 0, GRID_W - WIN_W)
    col_in = (col_ids[None, :] >= col_start[:, None]) & (
        col_ids[None, :] < col_start[:, None] + WIN_W
    )
    col_off = jnp.clip(col_ids[None, :] - col_ids[:, None], 1 - WIN_W, WIN_W - 1) + WIN_W - 1
    col_hot = (col_off[:, :, None] == jnp.arange(2 * WIN_W - 1)[None, None, :]).astype(jnp.float32)
    row_hot = (row_off[:, :, None] == jnp.arange(2 * WIN_H - 1)[None, None, :]).astype(jnp.float32)
    bias_table = lax.dynamic_slice_in_dim(rel_bias, lax.axis_index("tp") * head_dev, head_dev, 0)
    col_table = jnp.einsum("hec,qwc->heqw", bias_table, col_hot, precision=lax.Precision.HIGHEST)
    bias_win = jnp.einsum("rke,heqw->rqhkw", row_hot, col_table, precision=lax.Precision.HIGHEST)
    inv_scale = HEAD_DIM ** (-0.5)
    scores_win = (
        jnp.einsum("rqhd,rkwhd->rqhkw", queries, key_win, preferred_element_type=jnp.float32)
        * inv_scale
        + bias_win
    )
    scores_win = jnp.where(col_in[None, :, None, None, :], scores_win, NEG_BIG)
    scores_win = scores_win.reshape(grid_rows, GRID_W, head_dev, WIN_H * GRID_W)
    scores_ctx = (
        jnp.einsum("rqhd,chd->rqhc", queries, ctx_key3, preferred_element_type=jnp.float32)
        * inv_scale
    )
    row_max = jnp.maximum(jnp.max(scores_win, axis=-1), jnp.max(scores_ctx, axis=-1))
    exp_win = jnp.exp(scores_win - row_max[..., None])
    exp_ctx = jnp.exp(scores_ctx - row_max[..., None])
    row_total = jnp.sum(exp_win, axis=-1) + jnp.sum(exp_ctx, axis=-1)
    probs_win = (exp_win / row_total[..., None]).astype(jnp.bfloat16)
    probs_win = probs_win.reshape(grid_rows, GRID_W, head_dev, WIN_H, GRID_W)
    probs_ctx = (exp_ctx / row_total[..., None]).astype(jnp.bfloat16)
    attended = jnp.einsum(
        "rqhkw,rkwhd->rqhd", probs_win, val_win, preferred_element_type=jnp.float32
    )
    attended = attended + jnp.einsum(
        "rqhc,chd->rqhd", probs_ctx, ctx_val3, preferred_element_type=jnp.float32
    )
    attended = attended.astype(jnp.bfloat16).reshape(grid_rows * GRID_W, head_cols)
    branch = lax.psum_scatter(
        jnp.dot(attended, w_out, preferred_element_type=jnp.float32).astype(jnp.bfloat16),
        "tp",
        scatter_dimension=0,
        tiled=True,
    ).astype(jnp.float32)
    return (latent.astype(jnp.float32) + mod_vecs[4] * branch).astype(jnp.bfloat16)


def solution(mesh):
    placed = (
        P(("sp", "tp"), None),
        P("sp", None),
        P(),
        P(),
        P(),
        P("sp", "tp"),
        P("sp", "tp"),
        P("sp", "tp"),
        P(None, "tp"),
        P(None, "tp"),
        P(None, "tp"),
        P("tp", None),
        P(),
    )
    return jax.shard_map(
        on_device, mesh=mesh, in_specs=placed, out_specs=P(("sp", "tp"), None), check_vma=False
    )
```

profile of v0, /device:TPU:0, one launch (start us, length us, event | category | flops | bytes accessed | tf_op | source)
XLA Modules:
  0.0 193.7 jit_solution(12751256618278326930)
XLA Ops:
  6.6 0.8 fusion.61
  7.4 0.2 copy-done
  7.5 0.1 fusion.69
  7.7 1.1 fusion.70
  8.8 1.1 fusion.63
  9.9 42.3 %psum.7 = f32[5,2048]{1,0:T(8,128)S(1)} all-reduce(f32[5,2048]{1,0:T(8,128)S(1)} %maximum_dynamic-update-slice_fusion), channel_id=1, replica_groups=mesh['sp'=16,'tp'=2] {'sp','tp'}, use_global_device_ids=true, to_apply=%region_0.1 | all-reduce | flops 10240 | bytes 81920 | tf_op jit(solution)/shard_map/psum | solution.py:86
  52.2 1.2 fusion.35
  53.5 2.1 %fusion.39 = bf16[128,2048]{1,0:T(8,128)(2,1)} fusion(bf16[128,2048]{1,0:T(8,128)(2,1)} %param.13, f32[2048]{0:T(1024)S(1)} %bitcast.155, f32[2048]{0:T(1024)S(1)} %bitcast.156, f32[2048]{0:T(1024)} %param.17, f32[128]{0:T(128)S(1)} %add_rsqrt_fusion.1), kind=kLoop, calls=%fused_computation.46 | loop fusion | flops 1572864 | bytes 1073664 | tf_op jit(solution)/shard_map/convert_element_type | solution.py:39
  55.7 1.3 fusion.41
  57.0 3.2 %fusion.33 = bf16[1,64,1024]{2,1,0:T(8,128)(2,1)S(1)} fusion(bf16[2048,1024]{1,0:T(8,128)(2,1)} %param.22, bf16[64,2048]{1,0:T(8,128)(2,1)} %param.14, f32[2048]{0:T(1024)S(1)} %bitcast.150, f32[2048]{0:T(1024)S(1)} %bitcast.152, f32[2048]{0:T(1024)} %param.17, f32[64]{0:T(128)S(1)} %add_rsqrt_fusion), kind=kOutput, calls=%fused_computation.40 | convolution fusion | flops 269287424 | bytes 4612352 | tf_op jit(solution)/shard_map/dot_general | solution.py:45
  60.2 0.9 fusion.34
  61.1 0.7 pad_maximum_fusion.2
  62.1 1.4 fusion.51
  63.5 5.6 %fusion.12 = f32[8,32,32,8,8]{2,4,3,1,0:T(8,128)} fusion(f32[8,15,32,32]{3,1,2,0:T(8,128)S(1)} %fusion.51, s32[8,8]{1,0:T(8,128)S(1)} %subtract_add_fusion), kind=kOutput, calls=%fused_computation.21 | convolution fusion | flops 94372800 | bytes 2588928 | tf_op jit(solution)/shard_map/rke,heqw->rqhkw/dot_general | solution.py:134
  69.2 9.3 %copy.59 = f32[8,32,32,8,8]{1,2,4,0,3:T(8,128)} copy(f32[8,32,32,8,8]{2,4,3,1,0:T(8,128)} %fusion.12) | data formatting | bytes 4194304 | tf_op jit(solution)/shard_map/rke,heqw->rqhkw/dot_general | solution.py:134
  78.5 3.9 %convolution_convert_fusion.2 = bf16[256,1024]{1,0:T(8,128)(2,1)S(1)} fusion(bf16[256,2048]{1,0:T(8,128)(2,1)} %all-gather.3.cloned.1.call-done, bf16[2048,1024]{1,0:T(8,128)(2,1)} %param.23), kind=kOutput, calls=%fused_computation.35 | convolution fusion | flops 1074003968 | bytes 5767168 | tf_op jit(solution)/shard_map/dot_general | solution.py:45
  82.4 0.1 copy-done.10
  82.6 1.3 convolution_convert_fusion.3
  83.8 0.1 fusion.46
  83.9 4.2 %collective-permute-start = (bf16[2,4,32,1024]{3,2,0,1:T(8,128)(2,1)S(1)}, bf16[2,4,32,1024]{3,2,0,1:T(8,128)(2,1)S(1)}, u32[]{:S(2)}, u32[]{:S(2)}) collective-permute-start(bf16[2,4,32,1024]{3,2,0,1:T(8,128)(2,1)S(1)} %get-tuple-element.9), channel_id=1, source_target_pairs={{0,2},{2,4},{4,6},{6,8},{8,10},{10,12},{12,14},{14,16},{16,18},{18... | collective-permute-start | bytes 1572872 | tf_op jit(solution)/shard_map/ppermute | solution.py:25
  88.2 1.3 collective-permute-start.1
  89.5 1.3 fusion.32
  90.8 0.1 copy.82
  90.9 0.1 copy.61
  91.0 25.2 %collective-permute-done = bf16[2,4,32,1024]{3,2,0,1:T(8,128)(2,1)S(1)} collective-permute-done((bf16[2,4,32,1024]{3,2,0,1:T(8,128)(2,1)S(1)}, bf16[2,4,32,1024]{3,2,0,1:T(8,128)(2,1)S(1)}, u32[]{:S(2)}, u32[]{:S(2)}) %collective-permute-start) | collective-permute-done | bytes 524320 | tf_op jit(solution)/shard_map/ppermute | solution.py:25
  116.2 1.9 collective-permute-done.1
  118.1 0.3 pad_maximum_fusion
  118.4 4.9 %gather_fusion = bf16[8,2,8,32,1024]{4,3,1,2,0:T(8,128)(2,1)} fusion(bf16[2,16,32,1024]{3,2,0,1:T(8,128)(2,1)S(1)} %pad_maximum_fusion, s32[8]{0:T(128)S(1)} %shift-left_bitcast_fusion), kind=kCustom, calls=%fused_computation | custom fusion | bytes 16777344 | tf_op jit(solution)/shard_map/vmap()/gather | solution.py:111
  123.3 4.0 %fusion.66 = (bf16[8,1,8,32,1024]{4,3,1,2,0:T(8,128)(2,1)S(1)}, bf16[8,1,8,32,1024]{4,3,1,2,0:T(8,128)(2,1)S(1)}) fusion(bf16[8,2,8,32,1024]{4,3,1,2,0:T(8,128)(2,1)} %gather_fusion), kind=kLoop, calls=%fused_computation.99 | loop fusion | bytes 16777216 | tf_op jit(solution)/shard_map/slice | solution.py:115
  127.3 1.1 copy.81
  128.4 3.3 %copy.80 = bf16[256,8,8,128]{3,2,1,0:T(8,128)(2,1)} copy(bf16[256,8,8,128]{3,1,2,0:T(8,128)(2,1)S(1)} %bitcast.137) | data formatting | bytes 8388608
  131.7 1.2 slice-done.1
  132.9 4.3 %fusion.68 = (f32[8,32,8]{1,2,0:T(8,128)S(1)}, f32[8,32,8,8,32]{1,4,3,2,0:T(8,128)}) fusion(f32[8,32,32,8,8]{1,2,4,0,3:T(8,128)S(1)} %bitcast.133, bf16[8,32,8,128,1]{3,2,1,0,4:T(8,128)(2,1)S(1)} %bitcast_bitcast_fusion, bf16[8,8,32,8,128]{4,3,2,1,0:T(8,128)(2,1)S(1)} %bitcast.136, pred[32,32]{0,1:T(8,128)(4,1)S(1)} %fusion.57), kind=kOutput, calls=%fused_computation.101 | convolution fusion | flops 136312832 | bytes 8922112 | tf_op jit(solution)/shard_map/rqhd,rkwhd->rqhkw/dot_general | solution.py:137
  137.2 19.0 %all-gather.5.cloned.1.call-done = bf16[2,1024,1024]{2,1,0:T(8,128)(2,1)} async-done(((bf16[2,64,1024]{2,1,0:T(8,128)(2,1)}), bf16[2,1024,1024]{2,1,0:T(8,128)(2,1)}) %all-gather.5.cloned.1.call-update) | async-done | bytes 4194320 | tf_op jit(solution)/shard_map/all_gather | solution.py:89
  156.2 3.2 %slice_bitcast_fusion = (bf16[128,8,8,128]{3,1,2,0:T(8,128)(2,1)S(1)}, bf16[128,8,8,128]{3,1,2,0:T(8,128)(2,1)S(1)}) fusion(bf16[2,1024,1024]{2,1,0:T(8,128)(2,1)} %all-gather.5.cloned.1.call-done), kind=kLoop, calls=%fused_computation.18 | loop fusion | bytes 8388608
  159.4 0.6 copy.83
  160.0 1.3 fusion.16
  161.3 0.7 bitcast_reduce_fusion
  162.0 1.9 fusion.3
  163.9 1.0 slice-done.3
  164.9 2.0 %fusion.2 = f32[8,32,8]{1,2,0:T(8,128)S(1)} fusion(f32[8,32,8,8,32]{1,4,3,2,0:T(8,128)S(1)} %bitcast.135, f32[8,32,8]{1,2,0:T(8,128)S(1)} %copy_maximum_fusion), kind=kLoop, calls=%fused_computation.9 | loop fusion | flops 1046528 | bytes 2113536 | tf_op jit(solution)/shard_map/reduce_sum | solution.py:150
  167.0 0.6 copy.84
  167.6 3.3 %fusion.21 = f32[8,32,8,128]{3,1,2,0:T(8,128)S(1)} fusion(bf16[1024,8,128]{2,1,0:T(8,128)(2,1)S(1)} %bitcast.143, f32[8,32,8]{1,0,2:T(8,128)S(1)} %copy.67, f32[8,32,8]{1,0,2:T(8,128)S(1)} %copy.63, f32[8,1024,256]{1,2,0:S(1)} %fusion.16), kind=kOutput, calls=%fused_computation.31 | convolution fusion | flops 545259520 | bytes 11550720 | tf_op jit(solution)/shard_map/rqhc,chd->rqhd/dot_general | solution.py:157
  170.9 2.3 %fusion.29 = bf16[8,32,8,128]{3,1,2,0:T(8,128)(2,1)S(1)} fusion(f32[8,32,8,128]{3,1,2,0:T(8,128)S(1)} %fusion.21, f32[8,32,8,8,32]{1,4,3,2,0:T(8,128)S(1)} %bitcast.135, f32[8,32,8]{1,2,0:T(8,128)S(1)} %copy_add_fusion, f32[8,32,8]{1,2,0:T(8,128)S(1)} %copy_maximum_fusion, bf16[8,8,32,8,128]{4,3,2,1,0:T(8,128)(2,1)S(1)} %bitcast.142), kind=kOutput, calls=%fused_computation.33 | convolution fusion | flops 136314880 | bytes 7880704 | tf_op jit(solution)/shard_map/rqhkw,rkwhd->rqhd/dot_general | solution.py:154
  173.2 0.2 copy.70
  173.5 4.5 %convolution_convert_fusion = bf16[256,2048]{1,0:T(8,128)(2,1)} fusion(bf16[1024,2048]{1,0:T(8,128)(2,1)} %param.24, bf16[32,8,8,128]{3,2,1,0:T(8,128)(2,1)S(1)} %bitcast.149), kind=kOutput, calls=%fused_computation.17 | convolution fusion | flops 1074266112 | bytes 5767168 | tf_op jit(solution)/shard_map/dot_general | solution.py:162
  178.0 7.1 %reduce-scatter.2.cloned.1.call-done = bf16[128,2048]{1,0:T(8,128)(2,1)} async-done(((bf16[256,2048]{1,0:T(8,128)(2,1)}), bf16[128,2048]{1,0:T(8,128)(2,1)}) %reduce-scatter.2.cloned.1.call-update) | async-done | bytes 524304 | tf_op jit(solution)/shard_map/reduce_scatter | solution.py:161
  185.1 2.0 %fusion.40 = bf16[128,2048]{1,0:T(8,128)(2,1)} fusion(bf16[128,2048]{1,0:T(8,128)(2,1)S(1)} %copy-done.2, bf16[128,2048]{1,0:T(8,128)(2,1)} %reduce-scatter.2.cloned.1.call-done, f32[2048]{0:T(1024)S(1)} %bitcast.154), kind=kLoop, calls=%fused_computation.47 | loop fusion | flops 1310720 | bytes 1581056 | tf_op jit(solution)/shard_map/convert_element_type | solution.py:167
  (52 shorter events, 0.5 us)
Async XLA Ops:
  6.5 1.0 copy-start
  6.5 53.7 %copy-start.7 = (f32[2048]{0:T(1024)S(1)}, f32[2048]{0:T(1024)}, u32[]{:S(2)}) copy-start(f32[2048]{0:T(1024)} %param.17) | copy-start | bytes 24580
  6.5 53.7 %copy-start.6 = (bf16[64,2048]{1,0:T(8,128)(2,1)S(1)}, bf16[64,2048]{1,0:T(8,128)(2,1)}, u32[]{:S(2)}) copy-start(bf16[64,2048]{1,0:T(8,128)(2,1)} %param.14) | copy-start | bytes 786436
  6.5 72.0 %all-gather.3.cloned.1.call-start = ((), (), s32[]{:S(2)}) async-start(), calls=%async_computation.1 | async-start | bytes 1572864 | tf_op jit(solution)/shard_map/all_gather | solution.py:88
  55.6 100.6 %all-gather.5.cloned.1.call-start = ((), (), s32[]{:S(2)}) async-start(), calls=%async_computation.2 | async-start | bytes 4456448 | tf_op jit(solution)/shard_map/all_gather | solution.py:89
  55.7 4.6 %copy-start.3 = (bf16[2048,1024]{1,0:T(8,128)(2,1)S(1)}, bf16[2048,1024]{1,0:T(8,128)(2,1)}, u32[]{:S(2)}) copy-start(bf16[2048,1024]{1,0:T(8,128)(2,1)} %param.23) | copy-start | bytes 12582916
  56.9 5.0 %copy-start.8 = (f32[16,15,31]{2,0,1:T(8,128)S(1)}, f32[16,15,31]{2,0,1:T(8,128)}, u32[]{:S(2)}) copy-start(f32[16,15,31]{2,0,1:T(8,128)} %param.25) | copy-start | bytes 89284
  61.9 123.2 %reduce-scatter.2.cloned.1.call-start = ((), (), s32[]{:S(2)}) async-start(), calls=%async_computation.3 | async-start | bytes 1572864 | tf_op jit(solution)/shard_map/reduce_scatter | solution.py:161
  78.5 3.9 %copy-start.4 = (bf16[2048,1024]{1,0:T(8,128)(2,1)S(1)}, bf16[2048,1024]{1,0:T(8,128)(2,1)}, u32[]{:S(2)}) copy-start(bf16[2048,1024]{1,0:T(8,128)(2,1)} %param.22) | copy-start | bytes 12582916
  78.5 4.0 %copy-start.10 = (bf16[256,2048]{1,0:T(8,128)(2,1)S(1)}, bf16[256,2048]{1,0:T(8,128)(2,1)}, u32[]{:S(2)}) copy-start(bf16[256,2048]{1,0:T(8,128)(2,1)} %all-gather.3.cloned.1.call-done) | copy-start | bytes 3145732
  82.6 6.9 %copy-start.9 = (bf16[2048,1024]{1,0:T(8,128)(2,1)S(1)}, bf16[2048,1024]{1,0:T(8,128)(2,1)}, u32[]{:S(2)}) copy-start(bf16[2048,1024]{1,0:T(8,128)(2,1)} %param.21) | copy-start | bytes 12582916
  83.9 32.3 %collective-permute-start = (bf16[2,4,32,1024]{3,2,0,1:T(8,128)(2,1)S(1)}, bf16[2,4,32,1024]{3,2,0,1:T(8,128)(2,1)S(1)}, u32[]{:S(2)}, u32[]{:S(2)}) collective-permute-start(bf16[2,4,32,1024]{3,2,0,1:T(8,128)(2,1)S(1)} %get-tuple-element.9), channel_id=1, source_target_pairs={{0,2},{2,4},{4,6},{6,8},{8,10},{10,12},{12,14},{14,16},{16,18},{18... | collective-permute-start | bytes 1572872 | tf_op jit(solution)/shard_map/ppermute | solution.py:25
  88.2 30.0 %collective-permute-start.1 = (bf16[2,4,32,1024]{3,2,0,1:T(8,128)(2,1)S(1)}, bf16[2,4,32,1024]{3,2,0,1:T(8,128)(2,1)S(1)}, u32[]{:S(2)}, u32[]{:S(2)}) collective-permute-start(bf16[2,4,32,1024]{3,2,0,1:T(8,128)(2,1)S(1)} %get-tuple-element.10), channel_id=1, source_target_pairs={{2,0},{4,2},{6,4},{8,6},{10,8},{12,10},{14,12},{16,14},{18,16},{20... | collective-permute-start | bytes 1572872 | tf_op jit(solution)/shard_map/ppermute | solution.py:27
  127.3 4.5 %slice-start = ((s8[8388608]{0:T(1024)(128)(4,1)}), s8[4194304]{0:T(1024)(128)(4,1)S(1)}, s32[]{:S(2)}) async-start(s8[8388608]{0:T(1024)(128)(4,1)} %bitcast.132), calls=%async_computation.4 | async-start | bytes 8388608
  128.4 4.5 %slice-start.1 = ((s8[8388608]{0:T(1024)(128)(4,1)}), s8[4194304]{0:T(1024)(128)(4,1)S(1)}, s32[]{:S(2)}) async-start(s8[8388608]{0:T(1024)(128)(4,1)} %bitcast.132), calls=%async_computation.5 | async-start | bytes 8388608
  161.3 2.6 %slice-start.2 = ((s8[8388608]{0:T(1024)(128)(4,1)}), s8[4194304]{0:T(1024)(128)(4,1)S(1)}, s32[]{:S(2)}) async-start(s8[8388608]{0:T(1024)(128)(4,1)} %bitcast.134), calls=%async_computation.6 | async-start | bytes 8388608
  162.0 2.9 %slice-start.3 = ((s8[8388608]{0:T(1024)(128)(4,1)}), s8[4194304]{0:T(1024)(128)(4,1)S(1)}, s32[]{:S(2)}) async-start(s8[8388608]{0:T(1024)(128)(4,1)} %bitcast.134), calls=%async_computation.7 | async-start | bytes 8388608
  167.6 3.3 %copy-start.5 = (bf16[256,8,8,128]{3,2,1,0:T(8,128)(2,1)S(1)}, bf16[256,8,8,128]{3,2,1,0:T(8,128)(2,1)}, u32[]{:S(2)}) copy-start(bf16[256,8,8,128]{3,2,1,0:T(8,128)(2,1)} %copy.80) | copy-start | bytes 12582916
  173.5 11.7 %copy-start.2 = (bf16[128,2048]{1,0:T(8,128)(2,1)S(1)}, bf16[128,2048]{1,0:T(8,128)(2,1)}, u32[]{:S(2)}) copy-start(bf16[128,2048]{1,0:T(8,128)(2,1)} %param.13) | copy-start | bytes 1572868
  173.5 13.6 %copy-start.1 = (bf16[128,1024]{1,0:T(8,128)(2,1)S(1)}, bf16[128,1024]{1,0:T(8,128)(2,1)}, u32[]{:S(2)}) copy-start(bf16[128,1024]{1,0:T(8,128)(2,1)} %param.18) | copy-start | bytes 786436
Sparse Core Ops, SparseCore 0:
  55.7 8.8 all-gather.2
  67.3 88.8 all-gather.4
  178.1 6.9 reduce-scatter.1
where the time goes:
time: 194 us
  waiting for transfers between devices  53.3 us (27%)
  blocking collectives  42.3 us (22%)
  matrix products  35.6 us (18%)
  local copies, waits for them, and re-layouts  30 us (15%)
  between operations  13.6 us (7%)
  other arithmetic  13.3 us (7%)
  starting transfers between devices  5.61 us (3%)
    psum x1, blocking collectives, on_device(): mod_vecs = lax.psum(placed, ('sp', 'tp'))  42.3 us
    ppermute x1, waiting for transfers between devices, padded_2(): lax.ppermute(tail, axis, [(i, (i + 1) % count) for i in range(ends)])  25.2 us
    all_gather x1, waiting for transfers between devices, on_device(): lax.all_gather(project(rms_mod(context, norm_gain, mod_vecs[1], mod_vecs[...  19 us
    unnamed x36, local copies, waits for them, and re-layouts  11.5 us
    dot_general x5, matrix products, project(): jnp.dot(block, weight, preferred_element_type=jnp.float32)  10.6 us
    dot_general x1, local copies, waits for them, and re-layouts, on_device(): jnp.einsum('rke,heqw->rqhkw', row_hot, col_table, precision=lax.Precision...  9.27 us
    reduce_scatter x1, waiting for transfers between devices, on_device(): lax.psum_scatter(jnp.dot(attended, w_out, preferred_element_type=jnp.floa...  7.12 us
    dot_general x1, matrix products, on_device(): jnp.einsum('rke,heqw->rqhkw', row_hot, col_table, precision=lax.Precision...  5.61 us
  transfers between devices with their start and end apart: 5, of which 4 were waited for; matrix products, arithmetic and copies ran while one was open for 24% of the time, Pallas kernels for 0%

commit v1 on v0

v1 whole, which is shorter than its diff:
```python
import functools

import jax
import jax.numpy as jnp
from jax import lax
from jax.experimental import pallas as pl
from jax.experimental.pallas import tpu as pltpu
from jax.sharding import PartitionSpec as P

HEAD_DIM = 128
GRID_W = 32
WIN_H = 8
WIN_W = 16
HALF = WIN_H // 2
NORM_EPS = 1e-06
NEG_BIG = -1e30
MESH = pl.DeviceIdType.MESH
VMEM = pltpu.VMEM


def gather_kernel(
    sp, tp, act_ref, wsh_ref, wsc_ref, wg_ref, lat_ref, ctx_ref,
    mod_out, lat_out, ctx_out,
    part, mod_buf,
    m_send, m_recv, mf_send, mf_recv, own_send, own_recv,
    h_send, h_recv, hf_send, hf_recv, c_send, c_recv, cf_send, cf_recv, loc_sem,
):
    s = lax.axis_index("sp")
    t = lax.axis_index("tp")
    rows = lat_ref.shape[0]
    crow = ctx_ref.shape[0]
    cw = ctx_ref.shape[1] // tp
    tokens = rows * tp
    halo = tokens // 2

    def remote(src, dst, ss, rs, dev):
        return pltpu.make_async_remote_copy(
            src_ref=src, dst_ref=dst, send_sem=ss, recv_sem=rs,
            device_id=dev, device_id_type=MESH,
        )

    def sp_peer(d):
        return lax.rem(s + d, sp)

    def tp_peer(d):
        return lax.rem(t + d, tp)

    barrier = pltpu.get_barrier_semaphore()

    def greet(d, c):
        pl.semaphore_signal(barrier, inc=1, device_id=(sp_peer(d), t), device_id_type=MESH)
        return c

    lax.fori_loop(1, sp, greet, 0)
    for d in range(1, tp):
        pl.semaphore_signal(barrier, inc=1, device_id=(s, tp_peer(d)), device_id_type=MESH)

    def act(k):
        return act_ref[8 * k : 8 * k + 8, :].astype(jnp.bfloat16)

    val = (
        jnp.dot(act(0), wsh_ref[...], preferred_element_type=jnp.float32)
        + jnp.dot(act(1), wsc_ref[...], preferred_element_type=jnp.float32)
        + jnp.dot(act(2), wg_ref[...], preferred_element_type=jnp.float32)
    )
    part[...] = val
    mod_buf[pl.ds(s, 1)] = val[None]

    pl.semaphore_wait(barrier, sp - 1 + tp - 1)

    def mod_copy(d, src):
        return remote(part, mod_buf.at[src], m_send.at[d], m_recv.at[d], (sp_peer(d), t))

    def send_mod(d, c):
        mod_copy(d, s).start()
        return c

    lax.fori_loop(1, sp, send_mod, 0)

    def own_rows(who):
        return lat_out.at[pl.ds(pl.multiple_of(halo + who * rows, rows), rows), :]

    for d in range(1, tp):
        remote(lat_ref, own_rows(t), own_send.at[d], own_recv.at[d], (s, tp_peer(d))).start()
    local_lat = pltpu.make_async_copy(lat_ref, own_rows(t), loc_sem.at[0])
    local_lat.start()
    local_ctx = pltpu.make_async_copy(
        ctx_ref, ctx_out.at[pl.ds(pl.multiple_of(s * crow, crow), crow), :], loc_sem.at[1]
    )
    local_ctx.start()

    upper = t >= tp // 2

    def halo_rows(who):
        off = jnp.where(
            who >= tp // 2, (who - tp // 2) * rows, halo + tokens + who * rows
        )
        return lat_out.at[pl.ds(pl.multiple_of(off, rows), rows), :]

    halo_dev = jnp.where(upper, lax.rem(s + 1, sp), lax.rem(s + sp - 1, sp))
    halo_copy = remote(lat_ref, halo_rows(t), h_send, h_recv, (halo_dev, t))
    halo_copy.start()

    def ctx_block(src, who):
        return ctx_out.at[
            pl.ds(pl.multiple_of(src * crow, crow), crow),
            pl.ds(pl.multiple_of(who * cw, cw), cw),
        ]

    def ctx_copy(d, src):
        return remote(
            ctx_ref.at[:, pl.ds(pl.multiple_of(t * cw, cw), cw)],
            ctx_block(src, t), c_send.at[d], c_recv.at[d], (sp_peer(d), t),
        )

    def send_ctx(d, c):
        ctx_copy(d, s).start()
        return c

    lax.fori_loop(1, sp, send_ctx, 0)

    def recv_mod(d, c):
        mod_copy(d, lax.rem(s + sp - d, sp)).wait_recv()
        return c

    lax.fori_loop(1, sp, recv_mod, 0)
    mod_out[pl.ds(t, 1)] = jnp.sum(mod_buf[...], axis=0, keepdims=True)

    def mod_fwd(d, who):
        return remote(
            mod_out.at[who], mod_out.at[who], mf_send.at[d], mf_recv.at[d], (s, tp_peer(d))
        )

    for d in range(1, tp):
        mod_fwd(d, t).start()

    def halo_fwd(d, who):
        return remote(
            halo_rows(who), halo_rows(who), hf_send.at[d], hf_recv.at[d], (s, tp_peer(d))
        )

    halo_copy.wait_recv()
    for d in range(1, tp):
        halo_fwd(d, t).start()

    def ctx_fwd(d, e, src, who):
        return remote(
            ctx_block(src, who), ctx_block(src, who),
            cf_send.at[d, e], cf_recv.at[d, e], (s, tp_peer(e)),
        )

    def relay_ctx(d, c):
        src = lax.rem(s + sp - d, sp)
        ctx_copy(d, src).wait_recv()
        for e in range(1, tp):
            ctx_fwd(d, e, src, t).start()
        return c

    lax.fori_loop(1, sp, relay_ctx, 0)

    for d in range(1, tp):
        who = lax.rem(t + tp - d, tp)
        remote(lat_ref, own_rows(who), own_send.at[d], own_recv.at[d], (s, tp_peer(d))).wait()
        mod_fwd(d, who).wait()
        halo_fwd(d, who).wait()

    def finish(d, c):
        src = lax.rem(s + sp - d, sp)
        for e in range(1, tp):
            ctx_fwd(d, e, src, lax.rem(t + tp - e, tp)).wait()
        mod_copy(d, s).wait_send()
        ctx_copy(d, s).wait_send()
        return c

    lax.fori_loop(1, sp, finish, 0)
    halo_copy.wait_send()
    local_lat.wait()
    local_ctx.wait()


def gather_all(sp, tp, acts, w_shift, w_scale, w_gate, latent, context):
    width = latent.shape[1]
    cols = w_shift.shape[1]
    tokens = latent.shape[0] * tp
    dma = pltpu.SemaphoreType.DMA
    spec = pl.BlockSpec(memory_space=VMEM)
    return pl.pallas_call(
        functools.partial(gather_kernel, sp, tp),
        out_shape=(
            jax.ShapeDtypeStruct((tp, 8, cols), jnp.float32),
            jax.ShapeDtypeStruct((2 * tokens, width), jnp.bfloat16),
            jax.ShapeDtypeStruct((context.shape[0] * sp, width), jnp.bfloat16),
        ),
        in_specs=[spec] * 6,
        out_specs=(spec,) * 3,
        scratch_shapes=[
            VMEM((8, cols), jnp.float32),
            VMEM((sp, 8, cols), jnp.float32),
            dma((sp,)), dma((sp,)), dma((tp,)), dma((tp,)), dma((tp,)), dma((tp,)),
            dma, dma, dma((tp,)), dma((tp,)), dma((sp,)), dma((sp,)),
            dma((sp, tp)), dma((sp, tp)), dma((2,)),
        ],
        compiler_params=pltpu.CompilerParams(collective_id=0, has_side_effects=True),
        name="gather_all",
    )(acts, w_shift, w_scale, w_gate, latent, context)


def attend_kernel(sp, tokens, n_lat, q_ref, k_ref, v_ref, tab_ref, o_ref):
    rows = tokens // GRID_W
    lanes = lax.broadcasted_iota(jnp.int32, (GRID_W, 128), 1)
    cq = lax.broadcasted_iota(jnp.int32, (GRID_W, 128), 0)
    c2 = lanes % GRID_W
    cs = jnp.clip(cq - WIN_W // 2, 0, GRID_W - WIN_W)
    col_in = (c2 >= cs) & (c2 < cs + WIN_W)
    per = 128 // GRID_W
    groups = []
    for k in range(24 // per):
        acc = jnp.full((GRID_W, 128), NEG_BIG, jnp.float32)
        for g in range(per):
            row = jnp.broadcast_to(tab_ref[0, per * k + g : per * k + g + 1, :], (GRID_W, 128))
            shift = (GRID_W * g - (WIN_W - 1)) % 128
            rolled = pltpu.roll(row, shift, 1, stride=1, stride_axis=0)
            acc = jnp.where(lanes // GRID_W == g, rolled, acc)
        groups.append(jnp.where(col_in, acc, NEG_BIG))
    table = jnp.concatenate(groups, axis=1)
    total = table.shape[1]
    first = lax.axis_index("sp") * rows
    all_rows = rows * sp
    kr = lax.broadcasted_iota(jnp.int32, (GRID_W, n_lat), 1) // GRID_W
    strips = []
    for r in range(rows):
        shift = (rows - 1 - r) * GRID_W
        strip = table if shift == 0 else pltpu.roll(table, total - shift, 1)
        lo = jnp.clip(first + r - HALF, 0, all_rows - WIN_H) - first + HALF
        strips.append(jnp.where((kr >= lo) & (kr < lo + WIN_H), strip[:, :n_lat], NEG_BIG))
    bias = jnp.concatenate(strips, axis=0)
    scores = lax.dot_general(
        q_ref[...], k_ref[...], (((1,), (1,)), ((), ())), preferred_element_type=jnp.float32
    ) * (HEAD_DIM ** -0.5)
    win = scores[:, :n_lat] + bias
    ctx = scores[:, n_lat:]
    top = jnp.maximum(
        jnp.max(win, axis=1, keepdims=True), jnp.max(ctx, axis=1, keepdims=True)
    )
    e_win = jnp.exp(win - top)
    e_ctx = jnp.exp(ctx - top)
    denom = jnp.sum(e_win, axis=1, keepdims=True) + jnp.sum(e_ctx, axis=1, keepdims=True)
    probs = jnp.concatenate([e_win.astype(jnp.bfloat16), e_ctx.astype(jnp.bfloat16)], axis=1)
    out = jnp.dot(probs, v_ref[...], preferred_element_type=jnp.float32)
    o_ref[...] = (out / denom).astype(jnp.bfloat16)


def attend(sp, n_lat, queries, keys, values, table):
    tokens, cols = queries.shape
    kv = keys.shape[0]
    heads = cols // HEAD_DIM
    return pl.pallas_call(
        functools.partial(attend_kernel, sp, tokens, n_lat),
        grid=(heads,),
        out_shape=jax.ShapeDtypeStruct((tokens, cols), jnp.bfloat16),
        in_specs=[
            pl.BlockSpec((tokens, HEAD_DIM), lambda h: (0, h)),
            pl.BlockSpec((kv, HEAD_DIM), lambda h: (0, h)),
            pl.BlockSpec((kv, HEAD_DIM), lambda h: (0, h)),
            pl.BlockSpec((1, 24, 128), lambda h: (h, 0, 0)),
        ],
        out_specs=pl.BlockSpec((tokens, HEAD_DIM), lambda h: (0, h)),
        name="attend",
    )(queries, keys, values, table)


def output_kernel(tp, att_ref, w_ref, lat_ref, gate_ref, out_ref, sbuf, rbuf, send, recv):
    s = lax.axis_index("sp")
    t = lax.axis_index("tp")
    rows = lat_ref.shape[0]
    n_chunk = sbuf.shape[1]
    cw = sbuf.shape[3]
    barrier = pltpu.get_barrier_semaphore()
    for d in range(1, tp):
        pl.semaphore_signal(
            barrier, inc=1, device_id=(s, lax.rem(t + d, tp)), device_id_type=MESH
        )

    def product(who, c):
        a = att_ref[pl.ds(pl.multiple_of(who * rows, rows), rows), :]
        w = w_ref[:, c * cw : (c + 1) * cw]
        return jnp.dot(a, w, preferred_element_type=jnp.float32).astype(jnp.bfloat16)

    def copy(d, c):
        return pltpu.make_async_remote_copy(
            src_ref=sbuf.at[d, c], dst_ref=rbuf.at[d, c],
            send_sem=send.at[d, c], recv_sem=recv.at[d, c],
            device_id=(s, lax.rem(t + d, tp)), device_id_type=MESH,
        )

    for d in range(1, tp):
        for c in range(n_chunk):
            sbuf[d, c] = product(lax.rem(t + d, tp), c)
            if d == 1 and c == 0:
                pl.semaphore_wait(barrier, tp - 1)
            copy(d, c).start()
    for c in range(n_chunk):
        branch = product(t, c).astype(jnp.float32)
        for d in range(1, tp):
            copy(d, c).wait_recv()
            branch = branch + rbuf[d, c].astype(jnp.float32)
        sl = slice(c * cw, (c + 1) * cw)
        out_ref[:, sl] = (
            lat_ref[:, sl].astype(jnp.float32) + gate_ref[:, sl] * branch
        ).astype(jnp.bfloat16)
    for d in range(1, tp):
        for c in range(n_chunk):
            copy(d, c).wait_send()


def output(tp, attended, w_out, latent, gate):
    rows, width = latent.shape
    n_chunk = 4
    cw = width // n_chunk
    spec = pl.BlockSpec(memory_space=VMEM)
    dma = pltpu.SemaphoreType.DMA
    return pl.pallas_call(
        functools.partial(output_kernel, tp),
        out_shape=jax.ShapeDtypeStruct(latent.shape, jnp.bfloat16),
        in_specs=[spec] * 4,
        out_specs=spec,
        scratch_shapes=[
            VMEM((tp, n_chunk, rows, cw), jnp.bfloat16),
            VMEM((tp, n_chunk, rows, cw), jnp.bfloat16),
            dma((tp, n_chunk)), dma((tp, n_chunk)),
        ],
        compiler_params=pltpu.CompilerParams(collective_id=1, has_side_effects=True),
        name="output",
    )(attended, w_out, latent, gate)


def rms_mod(block, norm_gain, shifts, scales):
    block = block.astype(jnp.float32)
    normed = (
        block * lax.rsqrt(jnp.mean(block * block, axis=-1, keepdims=True) + NORM_EPS) * norm_gain
    )
    return (normed * (1.0 + scales) + shifts).astype(jnp.bfloat16)


def on_device(
    latent, context, condition, ctx_cond, norm_gain, w_shift, w_scale, w_gate,
    w_query, w_key, w_value, w_out, rel_bias,
):
    tp = lax.axis_size("tp")
    sp = lax.axis_size("sp")
    head_dev = w_query.shape[1] // HEAD_DIM
    row_part = w_shift.shape[0]
    tokens = latent.shape[0] * tp
    halo = HALF * GRID_W
    assert tokens == 2 * halo and tp % 2 == 0
    pair = jnp.stack([condition, ctx_cond])
    pair = lax.dynamic_slice_in_dim(pair, lax.axis_index("sp") * row_part, row_part, 1)
    activated = jax.nn.silu(pair).astype(jnp.bfloat16).astype(jnp.float32)
    acts = jnp.concatenate(
        [
            jnp.pad(activated, ((0, 6), (0, 0))),
            jnp.pad(activated, ((2, 4), (0, 0))),
            jnp.pad(activated[:1], ((4, 3), (0, 0))),
        ]
    )
    mod, lat_all, ctx_all = gather_all(
        sp, tp, acts, w_shift, w_scale, w_gate, latent, context
    )
    mod = jnp.concatenate([mod[i] for i in range(tp)], axis=1)
    normed = jnp.concatenate(
        [
            rms_mod(lat_all, norm_gain, mod[0], mod[2]),
            rms_mod(ctx_all, norm_gain, mod[1], mod[3]),
        ]
    )

    def proj(x, w):
        return jnp.dot(x, w, preferred_element_type=jnp.float32).astype(jnp.bfloat16)

    queries = proj(normed[halo : halo + tokens], w_query)
    keys = proj(normed, w_key)
    values = proj(normed, w_value)
    table = lax.dynamic_slice_in_dim(rel_bias, lax.axis_index("tp") * head_dev, head_dev, 0)
    table = jnp.pad(
        table, ((0, 0), (HALF, 24 - HALF - table.shape[1]), (0, 128 - table.shape[2]))
    )
    attended = attend(sp, 2 * tokens, queries, keys, values, table)
    return output(tp, attended, w_out, latent, mod[4:5])


def solution(mesh):
    placed = (
        P(("sp", "tp"), None),
        P("sp", None),
        P(),
        P(),
        P(),
        P("sp", "tp"),
        P("sp", "tp"),
        P("sp", "tp"),
        P(None, "tp"),
        P(None, "tp"),
        P(None, "tp"),
        P("tp", None),
        P(),
    )
    return jax.shard_map(
        on_device, mesh=mesh, in_specs=placed, out_specs=P(("sp", "tp"), None), check_vma=False
    )
```

time: 194 us -> 125 us (0.64)
  the two profiles are of different devices: /device:TPU:0 before, /device:TPU:31 now
where the time goes in v1:
time: 125 us
  Pallas kernels  91.8 us (73%)
  matrix products  20 us (16%)
  other arithmetic  8.42 us (7%)
  local copies, waits for them, and re-layouts  4.35 us (3%)
    pallas_call x1, Pallas kernels, gather_all(): pl.pallas_call(functools.partial(gather_kernel, sp, tp), out_shape=(jax.S...  75.1 us
    dot_general x3, matrix products, proj(): jnp.dot(x, w, preferred_element_type=jnp.float32).astype(jnp.bfloat16)  20 us
    pallas_call x1, Pallas kernels, attend(): pl.pallas_call(functools.partial(attend_kernel, sp, tokens, n_lat), grid=...  10.4 us
    pallas_call x1, Pallas kernels, output(): pl.pallas_call(functools.partial(output_kernel, tp), out_shape=jax.ShapeD...  6.29 us
    reduce_sum x2, other arithmetic, rms_mod(): jnp.mean(block * block, axis=-1, keepdims=True) + NORM_EPS  3.56 us
    convert_element_type x2, other arithmetic, rms_mod(): return (normed * (1.0 + scales) + shifts).astype(jnp.bfloat16)  2.81 us
    unnamed x16, local copies, waits for them, and re-layouts  2.74 us

profile of v1, /device:TPU:31, one launch (start us, length us, event | category | flops | bytes accessed | tf_op | source)
XLA Modules:
  0.0 124.6 jit_solution(10765332250433048560)
XLA Ops:
  0.0 0.0 copy-start
  0.0 0.0 copy-start.3
  0.0 0.8 fusion.18
  0.8 0.6 select_maximum_fusion.act_ref
  1.4 75.1 %gather_all.1 = (f32[2,8,1024]{2,1,0:T(8,128)}, bf16[512,2048]{1,0:T(8,128)(2,1)}, bf16[1024,2048]{1,0:T(8,128)(2,1)}) custom-call(f32[24,128]{1,0:T(8,128)} %select_maximum_fusion.act_ref, bf16[128,1024]{1,0:T(8,128)(2,1)} %wsh_ref.1, bf16[128,1024]{1,0:T(8,128)(2,1)} %wsc_ref.1, bf16[128,1024]{1,0:T(8,128)(2,1)} %wg_ref.1, bf16[128,2048]{1,0:T(8,128)(2,1)} %lat_ref.3, ...), custom_call_target="tpu_custom_call" | custom-call | tf_op jit(solution)/shard_map/gather_all/pallas_call | solution.py:187
  76.5 0.0 copy-start.1
  76.5 0.9 slice_bitcast_fusion.1
  77.4 0.6 pad_maximum_fusion.7
  78.1 3.1 %fusion = f32[1024]{0:T(1024)S(1)} fusion(bf16[1024,2048]{1,0:T(8,128)(2,1)} %get-tuple-element.10), kind=kLoop, calls=%fused_computation.2 | loop fusion | flops 6290432 | bytes 4198400 | tf_op jit(solution)/shard_map/reduce_sum | solution.py:340
  81.1 0.0 copy-done.3
  81.2 0.0 copy-done.1
  81.2 0.0 copy-start.2
  81.2 2.0 %fusion.4 = bf16[1024,2048]{1,0:T(8,128)(2,1)S(1)} fusion(bf16[1024,2048]{1,0:T(8,128)(2,1)S(1)} %copy-done.1, f32[2048]{0:T(1024)S(1)} %bitcast.15, f32[2048]{0:T(1024)S(1)} %bitcast.16, f32[2048]{0:T(1024)S(1)} %copy-done.3, f32[1024]{0:T(1024)S(1)} %add_rsqrt_fusion), kind=kLoop, calls=%fused_computation.6 | loop fusion | flops 12582912 | bytes 8417280 | tf_op jit(solution)/shard_map/convert_element_type | solution.py:342
  83.1 0.0 copy-start.4
  83.2 0.0 copy-done.2
  83.2 0.5 fusion.5
  83.7 0.9 fusion.9
  84.5 0.8 copy-done.4
  85.3 0.0 copy-start.5
  85.3 9.0 %fusion.13.v_ref = bf16[1536,1024]{1,0:T(8,128)(2,1)} fusion(bf16[2048,1024]{1,0:T(8,128)(2,1)S(1)} %copy-done.4, bf16[1024,2048]{1,0:T(8,128)(2,1)S(1)} %fusion.4, bf16[512,2048]{1,0:T(8,128)(2,1)S(1)} %fusion.9), kind=kOutput, calls=%fused_computation.18 | convolution fusion | flops 6456606720 | bytes 13631488 | tf_op jit(solution)/shard_map/dot_general | solution.py:378
  94.3 0.0 copy-done.5
  94.3 0.0 copy-start.6
  94.3 9.0 %fusion.12.k_ref = bf16[1536,1024]{1,0:T(8,128)(2,1)} fusion(bf16[2048,1024]{1,0:T(8,128)(2,1)S(1)} %copy-done.5, bf16[1024,2048]{1,0:T(8,128)(2,1)S(1)} %fusion.4, bf16[512,2048]{1,0:T(8,128)(2,1)S(1)} %fusion.9), kind=kOutput, calls=%fused_computation.17 | convolution fusion | flops 6456606720 | bytes 13631488 | tf_op jit(solution)/shard_map/dot_general | solution.py:378
  103.3 0.0 copy-done.6
  103.3 2.1 %convolution_convert_fusion.q_ref = bf16[256,1024]{1,0:T(8,128)(2,1)} fusion(bf16[2048,1024]{1,0:T(8,128)(2,1)S(1)} %copy-done.6, bf16[512,2048]{1,0:T(8,128)(2,1)S(1)} %fusion.9), kind=kOutput, calls=%fused_computation.19 | convolution fusion | flops 1074003968 | bytes 5767168 | tf_op jit(solution)/shard_map/dot_general | solution.py:378
  105.3 0.0 copy-done
  105.4 0.7 pad.19.tab_ref
  106.0 10.4 %attend.1.att_ref = bf16[256,1024]{1,0:T(8,128)(2,1)} custom-call(bf16[256,1024]{1,0:T(8,128)(2,1)} %convolution_convert_fusion.q_ref, bf16[1536,1024]{1,0:T(8,128)(2,1)} %fusion.12.k_ref, bf16[1536,1024]{1,0:T(8,128)(2,1)} %fusion.13.v_ref, f32[8,24,128]{2,1,0:T(8,128)} %pad.19.tab_ref), custom_call_target="tpu_custom_call" | custom-call | tf_op jit(solution)/shard_map/attend/pallas_call | solution.py:257
  116.5 6.3 %output.1 = bf16[128,2048]{1,0:T(8,128)(2,1)} custom-call(bf16[256,1024]{1,0:T(8,128)(2,1)} %attend.1.att_ref, bf16[1024,2048]{1,0:T(8,128)(2,1)} %w_ref.1, bf16[128,2048]{1,0:T(8,128)(2,1)} %lat_ref.3, f32[1,2048]{1,0:T(1,128)} %get-tuple-element.11.gate_ref), custom_call_target="tpu_custom_call" | custom-call | tf_op jit(solution)/shard_map/output/pallas_call | solution.py:322
  122.8 1.9 %copy.17 = bf16[128,2048]{1,0:T(8,128)(2,1)} copy(bf16[128,2048]{1,0:T(8,128)(2,1)} %output.1) | data formatting | bytes 1048576
  (5 shorter events, 0.0 us)
Async XLA Ops:
  0.0 105.3 %copy-start = (f32[16,15,31]{2,0,1:T(8,128)S(1)}, f32[16,15,31]{2,0,1:T(8,128)}, u32[]{:S(2)}) copy-start(f32[16,15,31]{2,0,1:T(8,128)} %param.25) | copy-start | bytes 89284
  0.0 81.1 %copy-start.3 = (f32[2048]{0:T(1024)S(1)}, f32[2048]{0:T(1024)}, u32[]{:S(2)}) copy-start(f32[2048]{0:T(1024)} %param.17) | copy-start | bytes 24580
  76.5 4.7 %copy-start.1 = (bf16[1024,2048]{1,0:T(8,128)(2,1)S(1)}, bf16[1024,2048]{1,0:T(8,128)(2,1)}, u32[]{:S(2)}) copy-start(bf16[1024,2048]{1,0:T(8,128)(2,1)} %get-tuple-element.10) | copy-start | bytes 12582916
  81.2 2.0 %copy-start.2 = (bf16[512,2048]{1,0:T(8,128)(2,1)S(1)}, bf16[512,2048]{1,0:T(8,128)(2,1)}, u32[]{:S(2)}) copy-start(bf16[512,2048]{1,0:T(8,128)(2,1)} %get-tuple-element.8) | copy-start | bytes 6291460
  83.1 2.2 %copy-start.4 = (bf16[2048,1024]{1,0:T(8,128)(2,1)S(1)}, bf16[2048,1024]{1,0:T(8,128)(2,1)}, u32[]{:S(2)}) copy-start(bf16[2048,1024]{1,0:T(8,128)(2,1)} %param.23) | copy-start | bytes 12582916
  85.3 9.0 %copy-start.5 = (bf16[2048,1024]{1,0:T(8,128)(2,1)S(1)}, bf16[2048,1024]{1,0:T(8,128)(2,1)}, u32[]{:S(2)}) copy-start(bf16[2048,1024]{1,0:T(8,128)(2,1)} %param.22) | copy-start | bytes 12582916
  94.3 9.0 %copy-start.6 = (bf16[2048,1024]{1,0:T(8,128)(2,1)S(1)}, bf16[2048,1024]{1,0:T(8,128)(2,1)}, u32[]{:S(2)}) copy-start(bf16[2048,1024]{1,0:T(8,128)(2,1)} %param.21) | copy-start | bytes 12582916

commit v2 on v1

--- a/solution.py
+++ b/solution.py
@@ -12,6 +12,7 @@
 WIN_H = 8
 WIN_W = 16
 HALF = WIN_H // 2
+INNER = 4
 NORM_EPS = 1e-06
 NEG_BIG = -1e30
 MESH = pl.DeviceIdType.MESH
@@ -21,15 +22,19 @@
 def gather_kernel(
     sp, tp, act_ref, wsh_ref, wsc_ref, wg_ref, lat_ref, ctx_ref,
     mod_out, lat_out, ctx_out,
-    part, mod_buf,
-    m_send, m_recv, mf_send, mf_recv, own_send, own_recv,
-    h_send, h_recv, hf_send, hf_recv, c_send, c_recv, cf_send, cf_recv, loc_sem,
+    in_buf, out_buf, mi_send, mi_recv, mo_send, mo_recv, mf_send, mf_recv,
+    own_send, own_recv, h_send, h_recv, hf_send, hf_recv,
+    z_send, z_recv, n_send, n_recv, d_send, d_recv, f_send, f_recv, loc_sem,
 ):
     s = lax.axis_index("sp")
     t = lax.axis_index("tp")
+    n_o = sp // INNER
+    o = s // INNER
+    i = lax.rem(s, INNER)
     rows = lat_ref.shape[0]
     crow = ctx_ref.shape[0]
     cw = ctx_ref.shape[1] // tp
+    hw = cw // 2
     tokens = rows * tp
     halo = tokens // 2
 
@@ -39,21 +44,38 @@
             device_id=dev, device_id_type=MESH,
         )
 
-    def sp_peer(d):
-        return lax.rem(s + d, sp)
+    def at(oo, ii):
+        return (oo * INNER + ii, t)
+
+    def outer(d):
+        return lax.rem(o + d, n_o)
+
+    def inner(d):
+        return lax.rem(i + d, INNER)
 
     def tp_peer(d):
         return lax.rem(t + d, tp)
 
+    ix = i + 1 - 2 * lax.rem(i, 2)
+    iy = lax.rem(i + 2, INNER)
+    ixy = lax.rem(ix + 2, INNER)
+    nbr = (ix, iy)
+    nxt = (lax.rem(s + 1, sp), t)
+    prv = (lax.rem(s + sp - 1, sp), t)
+
     barrier = pltpu.get_barrier_semaphore()
 
-    def greet(d, c):
-        pl.semaphore_signal(barrier, inc=1, device_id=(sp_peer(d), t), device_id_type=MESH)
-        return c
-
-    lax.fori_loop(1, sp, greet, 0)
-    for d in range(1, tp):
-        pl.semaphore_signal(barrier, inc=1, device_id=(s, tp_peer(d)), device_id_type=MESH)
+    def greet(dev):
+        pl.semaphore_signal(barrier, inc=1, device_id=dev, device_id_type=MESH)
+
+    for d in range(1, n_o):
+        greet(at(outer(d), i))
+    for d in range(1, INNER):
+        greet(at(o, inner(d)))
+    for d in range(1, tp):
+        greet((s, tp_peer(d)))
+    greet(nxt)
+    greet(prv)
 
     def act(k):
         return act_ref[8 * k : 8 * k + 8, :].astype(jnp.bfloat16)
@@ -63,25 +85,91 @@
         + jnp.dot(act(1), wsc_ref[...], preferred_element_type=jnp.float32)
         + jnp.dot(act(2), wg_ref[...], preferred_element_type=jnp.float32)
     )
-    part[...] = val
-    mod_buf[pl.ds(s, 1)] = val[None]
-
-    pl.semaphore_wait(barrier, sp - 1 + tp - 1)
-
-    def mod_copy(d, src):
-        return remote(part, mod_buf.at[src], m_send.at[d], m_recv.at[d], (sp_peer(d), t))
-
-    def send_mod(d, c):
-        mod_copy(d, s).start()
-        return c
-
-    lax.fori_loop(1, sp, send_mod, 0)
+    in_buf[pl.ds(i, 1)] = val[None]
+
+    pl.semaphore_wait(barrier, n_o - 1 + INNER - 1 + tp - 1 + 2)
+
+    def mod_in(d, who):
+        return remote(
+            in_buf.at[who], in_buf.at[who], mi_send.at[d], mi_recv.at[d], at(o, inner(d))
+        )
+
+    def mod_across(d, who):
+        return remote(
+            out_buf.at[who], out_buf.at[who], mo_send.at[d], mo_recv.at[d], at(outer(d), i)
+        )
+
+    def mod_fwd(d, who):
+        return remote(
+            mod_out.at[who], mod_out.at[who], mf_send.at[d], mf_recv.at[d], (s, tp_peer(d))
+        )
+
+    for d in range(1, INNER):
+        mod_in(d, i).start()
 
     def own_rows(who):
         return lat_out.at[pl.ds(pl.multiple_of(halo + who * rows, rows), rows), :]
 
-    for d in range(1, tp):
-        remote(lat_ref, own_rows(t), own_send.at[d], own_recv.at[d], (s, tp_peer(d))).start()
+    def own_copy(d, who):
+        return remote(lat_ref, own_rows(who), own_send.at[d], own_recv.at[d], (s, tp_peer(d)))
+
+    def halo_rows(who):
+        off = jnp.where(
+            who >= tp // 2, (who - tp // 2) * rows, halo + tokens + who * rows
+        )
+        return lat_out.at[pl.ds(pl.multiple_of(off, rows), rows), :]
+
+    halo_dev = (jnp.where(t >= tp // 2, nxt[0], prv[0]), t)
+    halo_copy = remote(lat_ref, halo_rows(t), h_send, h_recv, halo_dev)
+
+    def halo_fwd(d, who):
+        return remote(
+            halo_rows(who), halo_rows(who), hf_send.at[d], hf_recv.at[d], (s, tp_peer(d))
+        )
+
+    def block(oo, ii, who, half=None):
+        off = who * cw + (0 if half is None else half * hw)
+        size = cw if half is None else hw
+        return ctx_out.at[
+            pl.ds(pl.multiple_of((oo * INNER + ii) * crow, crow), crow),
+            pl.ds(pl.multiple_of(off, hw), size),
+        ]
+
+    mine = ctx_ref.at[:, pl.ds(pl.multiple_of(t * cw, cw), cw)]
+
+    def line(d, oo):
+        return remote(mine, block(oo, i, t), z_send.at[d], z_recv.at[d], at(outer(d), i))
+
+    def held(j):
+        return lax.rem(o + n_o - j, n_o)
+
+    def side(j, a, ii):
+        src = mine if j == 0 else block(held(j), ii, t)
+        return remote(
+            src, block(held(j), ii, t), n_send.at[j, a], n_recv.at[j, a], at(o, nbr[a])
+        )
+
+    def diag(j, a, ii):
+        ref = block(held(j), ii, t, a)
+        return remote(ref, ref, d_send.at[j, a], d_recv.at[j, a], at(o, nbr[1 - a]))
+
+    def share(e, j, k, who):
+        half = None if k < 3 else k - 3
+        ref = block(held(j), (i, ix, iy, ixy, ixy)[k], who, half)
+        return remote(
+            ref, ref, f_send.at[e, j, k], f_recv.at[e, j, k], (s, tp_peer(e))
+        )
+
+    def share_all(j, k):
+        for e in range(1, tp):
+            share(e, j, k, t).start()
+
+    for d in range(1, n_o):
+        line(d, o).start()
+    for a in range(2):
+        side(0, a, i).start()
+    for d in range(1, tp):
+        own_copy(d, t).start()
     local_lat = pltpu.make_async_copy(lat_ref, own_rows(t), loc_sem.at[0])
     local_lat.start()
     local_ctx = pltpu.make_async_copy(
@@ -89,90 +177,59 @@
     )
     local_ctx.start()
 
-    upper = t >= tp // 2
-
-    def halo_rows(who):
-        off = jnp.where(
-            who >= tp // 2, (who - tp // 2) * rows, halo + tokens + who * rows
-        )
-        return lat_out.at[pl.ds(pl.multiple_of(off, rows), rows), :]
-
-    halo_dev = jnp.where(upper, lax.rem(s + 1, sp), lax.rem(s + sp - 1, sp))
-    halo_copy = remote(lat_ref, halo_rows(t), h_send, h_recv, (halo_dev, t))
+    for d in range(1, INNER):
+        mod_in(d, lax.rem(i + INNER - d, INNER)).wait_recv()
+    out_buf[pl.ds(o, 1)] = jnp.sum(in_buf[...], axis=0, keepdims=True)
+    for d in range(1, n_o):
+        mod_across(d, o).start()
     halo_copy.start()
-
-    def ctx_block(src, who):
-        return ctx_out.at[
-            pl.ds(pl.multiple_of(src * crow, crow), crow),
-            pl.ds(pl.multiple_of(who * cw, cw), cw),
-        ]
-
-    def ctx_copy(d, src):
-        return remote(
-            ctx_ref.at[:, pl.ds(pl.multiple_of(t * cw, cw), cw)],
-            ctx_block(src, t), c_send.at[d], c_recv.at[d], (sp_peer(d), t),
-        )
-
-    def send_ctx(d, c):
-        ctx_copy(d, s).start()
-        return c
-
-    lax.fori_loop(1, sp, send_ctx, 0)
-
-    def recv_mod(d, c):
-        mod_copy(d, lax.rem(s + sp - d, sp)).wait_recv()
-        return c
-
-    lax.fori_loop(1, sp, recv_mod, 0)
-    mod_out[pl.ds(t, 1)] = jnp.sum(mod_buf[...], axis=0, keepdims=True)
-
-    def mod_fwd(d, who):
-        return remote(
-            mod_out.at[who], mod_out.at[who], mf_send.at[d], mf_recv.at[d], (s, tp_peer(d))
-        )
-
+    for d in range(1, n_o):
+        mod_across(d, held(d)).wait_recv()
+    mod_out[pl.ds(t, 1)] = jnp.sum(out_buf[...], axis=0, keepdims=True)
     for d in range(1, tp):
         mod_fwd(d, t).start()
 
-    def halo_fwd(d, who):
-        return remote(
-            halo_rows(who), halo_rows(who), hf_send.at[d], hf_recv.at[d], (s, tp_peer(d))
-        )
-
-    halo_copy.wait_recv()
-    for d in range(1, tp):
-        halo_fwd(d, t).start()
-
-    def ctx_fwd(d, e, src, who):
-        return remote(
-            ctx_block(src, who), ctx_block(src, who),
-            cf_send.at[d, e], cf_recv.at[d, e], (s, tp_peer(e)),
-        )
-
-    def relay_ctx(d, c):
-        src = lax.rem(s + sp - d, sp)
-        ctx_copy(d, src).wait_recv()
-        for e in range(1, tp):
-            ctx_fwd(d, e, src, t).start()
-        return c
-
-    lax.fori_loop(1, sp, relay_ctx, 0)
+    def relay(j):
+        for a in range(2):
+            side(j, a, nbr[a]).wait_recv()
+            diag(j, a, nbr[a]).start()
+            share_all(j, 1 + a)
+
+    for j in range(1, n_o):
+        line(j, held(j)).wait_recv()
+        for a in range(2):
+            side(j, a, i).start()
+        share_all(j, 0)
+        relay(j - 1)
+        if j == 1:
+            halo_copy.wait_recv()
+            for d in range(1, tp):
+                halo_fwd(d, t).start()
+    relay(n_o - 1)
+    for j in range(n_o):
+        for a in range(2):
+            diag(j, a, ixy).wait_recv()
+            share_all(j, 3 + a)
 
     for d in range(1, tp):
         who = lax.rem(t + tp - d, tp)
-        remote(lat_ref, own_rows(who), own_send.at[d], own_recv.at[d], (s, tp_peer(d))).wait()
+        own_copy(d, who).wait()
         mod_fwd(d, who).wait()
         halo_fwd(d, who).wait()
-
-    def finish(d, c):
-        src = lax.rem(s + sp - d, sp)
-        for e in range(1, tp):
-            ctx_fwd(d, e, src, lax.rem(t + tp - e, tp)).wait()
-        mod_copy(d, s).wait_send()
-        ctx_copy(d, s).wait_send()
-        return c
-
-    lax.fori_loop(1, sp, finish, 0)
+    for j in range(n_o):
+        for k in range(5):
+            if j == 0 and k == 0:
+                continue
+            for e in range(1, tp):
+                share(e, j, k, lax.rem(t + tp - e, tp)).wait()
+        for a in range(2):
+            side(j, a, i).wait_send()
+            diag(j, a, nbr[a]).wait_send()
+    for d in range(1, n_o):
+        line(d, o).wait_send()
+        mod_across(d, o).wait_send()
+    for d in range(1, INNER):
+        mod_in(d, i).wait_send()
     halo_copy.wait_send()
     local_lat.wait()
     local_ctx.wait()
@@ -182,6 +239,7 @@
     width = latent.shape[1]
     cols = w_shift.shape[1]
     tokens = latent.shape[0] * tp
+    n_o = sp // INNER
     dma = pltpu.SemaphoreType.DMA
     spec = pl.BlockSpec(memory_space=VMEM)
     return pl.pallas_call(
@@ -194,11 +252,12 @@
         in_specs=[spec] * 6,
         out_specs=(spec,) * 3,
         scratch_shapes=[
-            VMEM((8, cols), jnp.float32),
-            VMEM((sp, 8, cols), jnp.float32),
-            dma((sp,)), dma((sp,)), dma((tp,)), dma((tp,)), dma((tp,)), dma((tp,)),
-            dma, dma, dma((tp,)), dma((tp,)), dma((sp,)), dma((sp,)),
-            dma((sp, tp)), dma((sp, tp)), dma((2,)),
+            VMEM((INNER, 8, cols), jnp.float32),
+            VMEM((n_o, 8, cols), jnp.float32),
+            dma((INNER,)), dma((INNER,)), dma((n_o,)), dma((n_o,)), dma((tp,)), dma((tp,)),
+            dma((tp,)), dma((tp,)), dma, dma, dma((tp,)), dma((tp,)),
+            dma((n_o,)), dma((n_o,)), dma((n_o, 2)), dma((n_o, 2)),
+            dma((n_o, 2)), dma((n_o, 2)), dma((tp, n_o, 5)), dma((tp, n_o, 5)), dma((2,)),
         ],
         compiler_params=pltpu.CompilerParams(collective_id=0, has_side_effects=True),
         name="gather_all",
@@ -352,7 +411,7 @@
     row_part = w_shift.shape[0]
     tokens = latent.shape[0] * tp
     halo = HALF * GRID_W
-    assert tokens == 2 * halo and tp % 2 == 0
+    assert tokens == 2 * halo and tp % 2 == 0 and sp % INNER == 0
     pair = jnp.stack([condition, ctx_cond])
     pair = lax.dynamic_slice_in_dim(pair, lax.axis_index("sp") * row_part, row_part, 1)
     activated = jax.nn.silu(pair).astype(jnp.bfloat16).astype(jnp.float32)

time: 125 us -> 99.6 us (0.80)
  the two profiles are of different devices: /device:TPU:31 before, /device:TPU:0 now
where the time goes in v2:
time: 99.6 us; the launch traced here: 99.1 us
  Pallas kernels  66.3 us (67%)
  matrix products  20 us (20%)
  other arithmetic  8.42 us (8%)
  local copies, waits for them, and re-layouts  4.35 us (4%)
    pallas_call x1, Pallas kernels, gather_all(): pl.pallas_call(functools.partial(gather_kernel, sp, tp), out_shape=(jax.S...  49.5 us
    dot_general x3, matrix products, proj(): jnp.dot(x, w, preferred_element_type=jnp.float32).astype(jnp.bfloat16)  20 us
    pallas_call x1, Pallas kernels, attend(): pl.pallas_call(functools.partial(attend_kernel, sp, tokens, n_lat), grid=...  10.4 us
    pallas_call x1, Pallas kernels, output(): pl.pallas_call(functools.partial(output_kernel, tp), out_shape=jax.ShapeD...  6.32 us
    reduce_sum x2, other arithmetic, rms_mod(): jnp.mean(block * block, axis=-1, keepdims=True) + NORM_EPS  3.56 us
    convert_element_type x2, other arithmetic, rms_mod(): return (normed * (1.0 + scales) + shifts).astype(jnp.bfloat16)  2.81 us
    unnamed x16, local copies, waits for them, and re-layouts  2.74 us

profile of v2, /device:TPU:0, one launch (start us, length us, event | category | flops | bytes accessed | tf_op | source)
XLA Modules:
  0.0 99.1 jit_solution(14415025956763886859)
XLA Ops:
  0.0 0.0 copy-start
  0.0 0.0 copy-start.3
  0.0 0.8 fusion.18
  0.8 0.6 select_maximum_fusion.act_ref
  1.4 49.5 %gather_all.1 = (f32[2,8,1024]{2,1,0:T(8,128)}, bf16[512,2048]{1,0:T(8,128)(2,1)}, bf16[1024,2048]{1,0:T(8,128)(2,1)}) custom-call(f32[24,128]{1,0:T(8,128)} %select_maximum_fusion.act_ref, bf16[128,1024]{1,0:T(8,128)(2,1)} %wsh_ref.1, bf16[128,1024]{1,0:T(8,128)(2,1)} %wsc_ref.1, bf16[128,1024]{1,0:T(8,128)(2,1)} %wg_ref.1, bf16[128,2048]{1,0:T(8,128)(2,1)} %lat_ref.3, ...), custom_call_target="tpu_custom_call" | custom-call | tf_op jit(solution)/shard_map/gather_all/pallas_call | solution.py:245
  51.0 0.0 copy-start.1
  51.0 0.9 slice_bitcast_fusion.1
  51.9 0.6 pad_maximum_fusion.7
  52.5 3.1 %fusion = f32[1024]{0:T(1024)S(1)} fusion(bf16[1024,2048]{1,0:T(8,128)(2,1)} %get-tuple-element.10), kind=kLoop, calls=%fused_computation.2 | loop fusion | flops 6290432 | bytes 4198400 | tf_op jit(solution)/shard_map/reduce_sum | solution.py:399
  55.6 0.0 copy-done.3
  55.6 0.0 copy-done.1
  55.6 0.0 copy-start.2
  55.6 2.0 %fusion.4 = bf16[1024,2048]{1,0:T(8,128)(2,1)S(1)} fusion(bf16[1024,2048]{1,0:T(8,128)(2,1)S(1)} %copy-done.1, f32[2048]{0:T(1024)S(1)} %bitcast.15, f32[2048]{0:T(1024)S(1)} %bitcast.16, f32[2048]{0:T(1024)S(1)} %copy-done.3, f32[1024]{0:T(1024)S(1)} %add_rsqrt_fusion), kind=kLoop, calls=%fused_computation.6 | loop fusion | flops 12582912 | bytes 8417280 | tf_op jit(solution)/shard_map/convert_element_type | solution.py:401
  57.6 0.0 copy-start.4
  57.6 0.0 copy-done.2
  57.6 0.5 fusion.5
  58.1 0.9 fusion.9
  59.0 0.8 copy-done.4
  59.8 0.0 copy-start.5
  59.8 9.0 %fusion.13.v_ref = bf16[1536,1024]{1,0:T(8,128)(2,1)} fusion(bf16[2048,1024]{1,0:T(8,128)(2,1)S(1)} %copy-done.4, bf16[1024,2048]{1,0:T(8,128)(2,1)S(1)} %fusion.4, bf16[512,2048]{1,0:T(8,128)(2,1)S(1)} %fusion.9), kind=kOutput, calls=%fused_computation.18 | convolution fusion | flops 6456606720 | bytes 13631488 | tf_op jit(solution)/shard_map/dot_general | solution.py:437
  68.8 0.0 copy-done.5
  68.8 0.0 copy-start.6
  68.8 9.0 %fusion.12.k_ref = bf16[1536,1024]{1,0:T(8,128)(2,1)} fusion(bf16[2048,1024]{1,0:T(8,128)(2,1)S(1)} %copy-done.5, bf16[1024,2048]{1,0:T(8,128)(2,1)S(1)} %fusion.4, bf16[512,2048]{1,0:T(8,128)(2,1)S(1)} %fusion.9), kind=kOutput, calls=%fused_computation.17 | convolution fusion | flops 6456606720 | bytes 13631488 | tf_op jit(solution)/shard_map/dot_general | solution.py:437
  77.7 0.0 copy-done.6
  77.7 2.1 %convolution_convert_fusion.q_ref = bf16[256,1024]{1,0:T(8,128)(2,1)} fusion(bf16[2048,1024]{1,0:T(8,128)(2,1)S(1)} %copy-done.6, bf16[512,2048]{1,0:T(8,128)(2,1)S(1)} %fusion.9), kind=kOutput, calls=%fused_computation.19 | convolution fusion | flops 1074003968 | bytes 5767168 | tf_op jit(solution)/shard_map/dot_general | solution.py:437
  79.8 0.0 copy-done
  79.8 0.7 pad.19.tab_ref
  80.5 10.4 %attend.1.att_ref = bf16[256,1024]{1,0:T(8,128)(2,1)} custom-call(bf16[256,1024]{1,0:T(8,128)(2,1)} %convolution_convert_fusion.q_ref, bf16[1536,1024]{1,0:T(8,128)(2,1)} %fusion.12.k_ref, bf16[1536,1024]{1,0:T(8,128)(2,1)} %fusion.13.v_ref, f32[8,24,128]{2,1,0:T(8,128)} %pad.19.tab_ref), custom_call_target="tpu_custom_call" | custom-call | tf_op jit(solution)/shard_map/attend/pallas_call | solution.py:316
  90.9 6.3 %output.1 = bf16[128,2048]{1,0:T(8,128)(2,1)} custom-call(bf16[256,1024]{1,0:T(8,128)(2,1)} %attend.1.att_ref, bf16[1024,2048]{1,0:T(8,128)(2,1)} %w_ref.1, bf16[128,2048]{1,0:T(8,128)(2,1)} %lat_ref.3, f32[1,2048]{1,0:T(1,128)} %get-tuple-element.11.gate_ref), custom_call_target="tpu_custom_call" | custom-call | tf_op jit(solution)/shard_map/output/pallas_call | solution.py:381
  97.3 1.9 %copy.17 = bf16[128,2048]{1,0:T(8,128)(2,1)} copy(bf16[128,2048]{1,0:T(8,128)(2,1)} %output.1) | data formatting | bytes 1048576
  (5 shorter events, 0.0 us)
Async XLA Ops:
  0.0 79.8 %copy-start = (f32[16,15,31]{2,0,1:T(8,128)S(1)}, f32[16,15,31]{2,0,1:T(8,128)}, u32[]{:S(2)}) copy-start(f32[16,15,31]{2,0,1:T(8,128)} %param.25) | copy-start | bytes 89284
  0.0 55.6 %copy-start.3 = (f32[2048]{0:T(1024)S(1)}, f32[2048]{0:T(1024)}, u32[]{:S(2)}) copy-start(f32[2048]{0:T(1024)} %param.17) | copy-start | bytes 24580
  51.0 4.7 %copy-start.1 = (bf16[1024,2048]{1,0:T(8,128)(2,1)S(1)}, bf16[1024,2048]{1,0:T(8,128)(2,1)}, u32[]{:S(2)}) copy-start(bf16[1024,2048]{1,0:T(8,128)(2,1)} %get-tuple-element.10) | copy-start | bytes 12582916
  55.6 2.0 %copy-start.2 = (bf16[512,2048]{1,0:T(8,128)(2,1)S(1)}, bf16[512,2048]{1,0:T(8,128)(2,1)}, u32[]{:S(2)}) copy-start(bf16[512,2048]{1,0:T(8,128)(2,1)} %get-tuple-element.8) | copy-start | bytes 6291460
  57.6 2.2 %copy-start.4 = (bf16[2048,1024]{1,0:T(8,128)(2,1)S(1)}, bf16[2048,1024]{1,0:T(8,128)(2,1)}, u32[]{:S(2)}) copy-start(bf16[2048,1024]{1,0:T(8,128)(2,1)} %param.23) | copy-start | bytes 12582916
  59.8 9.0 %copy-start.5 = (bf16[2048,1024]{1,0:T(8,128)(2,1)S(1)}, bf16[2048,1024]{1,0:T(8,128)(2,1)}, u32[]{:S(2)}) copy-start(bf16[2048,1024]{1,0:T(8,128)(2,1)} %param.22) | copy-start | bytes 12582916
  68.8 9.0 %copy-start.6 = (bf16[2048,1024]{1,0:T(8,128)(2,1)S(1)}, bf16[2048,1024]{1,0:T(8,128)(2,1)}, u32[]{:S(2)}) copy-start(bf16[2048,1024]{1,0:T(8,128)(2,1)} %param.21) | copy-start | bytes 12582916
